TPU v7x, 32 devices: a whole 2x2x4 slice. The times are simulated.
32 devices in a mesh: sp: 16 (over z, y, x), tp: 2 (over core).
Axes of the slice: x: 2, y: 2, z: 4, core: 2. Of those that a mesh axis runs over, the one named last changes fastest.
Arguments:
- queries: bfloat16 [1, 6144, 2048], P(None, 'sp', 'tp'), may hold values from -5 to 5
- keys: bfloat16 [1, 6144, 2048], P(None, 'sp', 'tp'), may hold values from -5 to 5
- values: bfloat16 [1, 6144, 2048], P(None, 'sp', 'tp'), may hold values from -6 to 6
- rel_bias: float32 [16, 192], P('tp'), may hold values from -3 to 3
- out_grad: bfloat16 [1, 6144, 2048], P(None, 'sp', 'tp'), may hold values from -48 to 48
Outputs:
- query_grad: bfloat16 [1, 6144, 2048], P(None, 'sp', 'tp')
- key_grad: bfloat16 [1, 6144, 2048], P(None, 'sp', 'tp')
- value_grad: bfloat16 [1, 6144, 2048], P(None, 'sp', 'tp')
- bias_grad: float32 [16, 192], replicated
All inputs are finite; a program needn't handle non-finite values.
Results may differ from a plain program's by a relative error of at most 0.0049.
Values may be sent and summed in bfloat16 or wider, within the bound.
A program may use at most 64 MiB of HBM per device.

v0:
```python
import jax
import jax.numpy as jnp
from jax import lax
from jax.sharding import PartitionSpec as P

HEAD_DIM = 128
SEG = 64
LEFT = 4
CLIP = 128
BAND = 320
BUCKETS = 192


def from_behind(value, axis, steps):
    count = lax.axis_size(axis)
    leading, last = (max(0, -steps), min(count, count - steps))
    return lax.ppermute(value, axis, [(source, source + steps) for source in range(leading, last)])


def diagonal_onehot():
    span = SEG + BAND - 1
    diag = jnp.arange(span, dtype=jnp.int32)
    bucket = jnp.clip(SEG - 1 - diag + LEFT * SEG, 1 - SEG, CLIP) + SEG - 1
    return (bucket[None, :] == jnp.arange(BUCKETS, dtype=jnp.int32)[:, None]).astype(jnp.float32)


def on_diagonals(rel_bias, onehot):
    return jnp.dot(
        rel_bias, onehot, preferred_element_type=jnp.float32, precision=lax.Precision.HIGHEST
    )


def fill_toeplitz(diag_vals):
    head_count, span = diag_vals.shape
    tiled = jnp.tile(diag_vals, (1, SEG))[:, SEG - 1 :]
    tiled = tiled[:, : SEG * (span - 1)].reshape(head_count, SEG, span - 1)
    return tiled[:, :, :BAND]


def sum_diagonals(terms):
    head_count = terms.shape[0]
    span = SEG + BAND - 1
    padded = jnp.concatenate(
        [
            jnp.zeros((head_count, SEG, SEG - 1), jnp.float32),
            terms,
            jnp.zeros((head_count, SEG, SEG), jnp.float32),
        ],
        axis=2,
    )
    width = padded.shape[2]
    flat = jnp.concatenate(
        [padded.reshape(head_count, SEG * width), jnp.zeros((head_count, SEG), jnp.float32)], axis=1
    )
    skewed = flat.reshape(head_count, SEG, width + 1)[:, :, :span]
    return jnp.sum(skewed, axis=1)


def band_core(q_segs, k_band, v_band, g_segs, table, key_valid):
    seg_count = q_segs.shape[1]
    score_scale = HEAD_DIM ** (-0.5)
    score_parts = []
    prob_parts = []
    for offset in range(LEFT + 1):
        score_parts.append(
            jnp.einsum(
                "sncha,snkha->snhck",
                q_segs,
                k_band[:, offset : offset + seg_count],
                preferred_element_type=jnp.float32,
            )
        )
        prob_parts.append(
            jnp.einsum(
                "sncha,snkha->snhck",
                g_segs,
                v_band[:, offset : offset + seg_count],
                preferred_element_type=jnp.float32,
            )
        )
    score = jnp.concatenate(score_parts, axis=-1) * score_scale + table[None, None]
    score = jnp.where(key_valid[None, :, None, None, :], score, -jnp.inf)
    row_max = jnp.max(score, axis=-1, keepdims=True)
    expo = jnp.exp(score - row_max)
    row_sum = jnp.sum(expo, axis=-1, keepdims=True)
    prob = expo / row_sum
    log_norm = (row_max + jnp.log(row_sum))[..., 0]
    prob_grad = jnp.concatenate(prob_parts, axis=-1)
    row_delta = jnp.sum(prob * prob_grad, axis=-1)
    score_grad = prob * (prob_grad - row_delta[..., None])
    bias_terms = jnp.sum(score_grad, axis=(0, 1))
    prob_low = prob.astype(jnp.bfloat16)
    grad_low = (score_grad * score_scale).astype(jnp.bfloat16)
    query_acc = jnp.zeros(q_segs.shape, jnp.float32)
    key_acc = jnp.zeros(k_band.shape, jnp.float32)
    value_acc = jnp.zeros(k_band.shape, jnp.float32)
    for offset in range(LEFT + 1):
        grad_part = grad_low[..., offset * SEG : (offset + 1) * SEG]
        prob_part = prob_low[..., offset * SEG : (offset + 1) * SEG]
        query_acc = query_acc + jnp.einsum(
            "snhck,snkha->sncha",
            grad_part,
            k_band[:, offset : offset + seg_count],
            preferred_element_type=jnp.float32,
        )
        first_seg = 0
        key_acc = key_acc.at[:, offset + first_seg : offset + seg_count].add(
            jnp.einsum("snhck,sncha->snkha", grad_part, q_segs, preferred_element_type=jnp.float32)
        )
        value_acc = value_acc.at[:, offset + first_seg : offset + seg_count].add(
            jnp.einsum("snhck,sncha->snkha", prob_part, g_segs, preferred_element_type=jnp.float32)
        )
    return (query_acc, key_acc, value_acc, bias_terms, log_norm, row_delta)


def local(queries, keys, values, rel_bias, out_grad):
    seq_count, tok_rows, row_width = queries.shape
    head_count = row_width // HEAD_DIM
    seg_count = tok_rows // SEG
    reach = LEFT * SEG
    seq_index = lax.axis_index("sp")
    seg_shape = (seq_count, seg_count, SEG, head_count, HEAD_DIM)
    band_shape = (seq_count, seg_count + LEFT, SEG, head_count, HEAD_DIM)
    onehot = diagonal_onehot()
    table = fill_toeplitz(on_diagonals(rel_bias, onehot))
    prior_k, prior_v = from_behind(
        (keys[:, tok_rows - reach :], values[:, tok_rows - reach :]), "sp", 1
    )
    k_band = jnp.concatenate([prior_k, keys], axis=1).reshape(band_shape)
    v_band = jnp.concatenate([prior_v, values], axis=1).reshape(band_shape)
    q_segs = queries.reshape(seg_shape)
    g_segs = out_grad.reshape(seg_shape)
    positions = (
        seq_index * tok_rows
        + jnp.arange(seg_count, dtype=jnp.int32)[:, None] * SEG
        - reach
        + jnp.arange(BAND, dtype=jnp.int32)[None, :]
    )
    key_valid = positions >= 0
    flat = (seq_count, reach + tok_rows, row_width)
    query_acc, key_acc, value_acc, bias_terms, log_norm, row_delta = band_core(
        q_segs, k_band, v_band, g_segs, table, key_valid
    )
    key_flat = key_acc.reshape(flat)
    value_flat = value_acc.reshape(flat)
    back_k, back_v = from_behind((key_flat[:, :reach], value_flat[:, :reach]), "sp", -1)
    key_own = key_flat[:, reach:].at[:, tok_rows - reach :].add(back_k)
    value_own = value_flat[:, reach:].at[:, tok_rows - reach :].add(back_v)
    query_grad = query_acc.astype(jnp.bfloat16).reshape(seq_count, tok_rows, row_width)
    key_grad = key_own.astype(jnp.bfloat16)
    value_grad = value_own.astype(jnp.bfloat16)
    local_bias = jnp.dot(
        sum_diagonals(bias_terms),
        onehot.T,
        preferred_element_type=jnp.float32,
        precision=lax.Precision.HIGHEST,
    )
    full_table = jnp.zeros((head_count * lax.axis_size("tp"), BUCKETS), jnp.float32)
    full_table = lax.dynamic_update_slice_in_dim(
        full_table, local_bias, lax.axis_index("tp") * head_count, 0
    )
    bias_grad = lax.psum(full_table, ("sp", "tp"))
    return (query_grad, key_grad, value_grad, bias_grad)


def solution(mesh):
    return jax.shard_map(
        local,
        mesh=mesh,
        in_specs=(
            P(None, "sp", "tp"),
            P(None, "sp", "tp"),
            P(None, "sp", "tp"),
            P("tp", None),
            P(None, "sp", "tp"),
        ),
        out_specs=(P(None, "sp", "tp"), P(None, "sp", "tp"), P(None, "sp", "tp"), P()),
        check_vma=False,
    )
```

profile of v0, /device:TPU:0, one launch (start us, length us, event | category | flops | bytes accessed | tf_op | source)
XLA Modules:
  0.0 184.4 jit_solution(14857570000628562760)
XLA Ops:
  0.7 2.0 %slice.478 = bf16[1,256,1024]{2,1,0:T(8,128)(2,1)} slice(bf16[1,384,1024]{2,1,0:T(8,128)(2,1)} %param.30), slice={[0:1], [128:384], [0:1024]} | slice | bytes 1048576 | tf_op jit(solution)/shard_map/slice | solution.py:127
  2.7 5.7 %collective-permute-start = (bf16[1,256,1024]{2,1,0:T(8,128)(2,1)}, bf16[1,256,1024]{2,1,0:T(8,128)(2,1)}, u32[]{:S(2)}, u32[]{:S(2)}) collective-permute-start(bf16[1,256,1024]{2,1,0:T(8,128)(2,1)} %slice.478), channel_id=1, source_target_pairs={{0,2},{2,4},{4,6},{6,8},{8,10},{10,12},{12,14},{14,16},{16,18},{18... | collective-permute-start | bytes 1572872 | tf_op jit(solution)/shard_map/ppermute | solution.py:17
  8.3 1.9 %slice.486 = bf16[1,256,1024]{2,1,0:T(8,128)(2,1)} slice(bf16[1,384,1024]{2,1,0:T(8,128)(2,1)} %param.31), slice={[0:1], [128:384], [0:1024]} | slice | bytes 1048576 | tf_op jit(solution)/shard_map/slice | solution.py:127
  10.2 3.4 %collective-permute-start.1 = (bf16[1,256,1024]{2,1,0:T(8,128)(2,1)}, bf16[1,256,1024]{2,1,0:T(8,128)(2,1)}, u32[]{:S(2)}, u32[]{:S(2)}) collective-permute-start(bf16[1,256,1024]{2,1,0:T(8,128)(2,1)} %slice.486), channel_id=1, source_target_pairs={{0,2},{2,4},{4,6},{6,8},{8,10},{10,12},{12,14},{14,16},{16,18},{18... | collective-permute-start | bytes 1572872 | tf_op jit(solution)/shard_map/ppermute | solution.py:17
  16.0 2.0 %reshape.1124 = f32[8,64,382]{2,1,0:T(8,128)S(1)} reshape(f32[8,24448]{1,0:T(8,128)} %slice.522) | data formatting | bytes 1564672 | tf_op jit(solution)/shard_map/reshape | solution.py:36
  18.1 2.1 %collective-permute-done = bf16[1,256,1024]{2,1,0:T(8,128)(2,1)} collective-permute-done((bf16[1,256,1024]{2,1,0:T(8,128)(2,1)}, bf16[1,256,1024]{2,1,0:T(8,128)(2,1)}, u32[]{:S(2)}, u32[]{:S(2)}) %collective-permute-start) | collective-permute-done | bytes 524320 | tf_op jit(solution)/shard_map/ppermute | solution.py:17
  22.8 7.4 %collective-permute-done.1 = bf16[1,256,1024]{2,1,0:T(8,128)(2,1)} collective-permute-done((bf16[1,256,1024]{2,1,0:T(8,128)(2,1)}, bf16[1,256,1024]{2,1,0:T(8,128)(2,1)}, u32[]{:S(2)}, u32[]{:S(2)}) %collective-permute-start.1) | collective-permute-done | bytes 524320 | tf_op jit(solution)/shard_map/ppermute | solution.py:17
  44.5 1.8 convolution_bitcast_fusion.9
  49.7 6.9 %concatenate.116 = f32[1,6,8,64,320]{4,3,2,1,0:T(8,128)} concatenate(f32[1,6,8,64,64]{4,3,2,1,0:T(8,128)} %convolution_bitcast_fusion.11, f32[1,6,8,64,64]{4,3,2,1,0:T(8,128)} %convolution_bitcast_fusion.10, f32[1,6,8,64,64]{4,3,2,1,0:T(8,128)} %convolution_bitcast_fusion.9, f32[1,6,8,64,64]{4,3,2,1,0:T(8,128)} %convolution_bitcast_fusion.8, ...), dimensions={4} | concatenate | bytes 7864320 | tf_op jit(solution)/shard_map/concatenate | solution.py:81
  56.7 3.4 %fusion.2 = f32[6,8,64]{2,1,0:T(8,128)S(1)} fusion(f32[1,6,8,64,320]{4,3,2,1,0:T(8,128)} %concatenate.116, f32[8,64,320]{2,1,0:T(8,128)S(1)} %bitcast.227, pred[6,320]{1,0:T(8,128)(4,1)S(1)} %add_compare_fusion), kind=kLoop, calls=%fused_computation.7 | loop fusion | flops 3929088 | bytes 4601728 | tf_op jit(solution)/shard_map/reduce_max | solution.py:83
  62.1 7.0 %concatenate.123 = f32[1,6,8,64,320]{4,3,2,1,0:T(8,128)} concatenate(f32[1,6,8,64,64]{4,3,2,1,0:T(8,128)} %convolution_bitcast_fusion.6, f32[1,6,8,64,64]{4,3,2,1,0:T(8,128)} %convolution_bitcast_fusion.5, f32[1,6,8,64,64]{4,3,2,1,0:T(8,128)} %convolution_bitcast_fusion.4, f32[1,6,8,64,64]{4,3,2,1,0:T(8,128)} %convolution_bitcast_fusion.3, ...), dimensions={4} | concatenate | bytes 7864320 | tf_op jit(solution)/shard_map/concatenate | solution.py:88
  69.1 4.9 %multiply_reduce_fusion = f32[6,8,64]{2,1,0:T(8,128)S(1)} fusion(f32[1,6,8,64,320]{4,3,2,1,0:T(8,128)} %concatenate.123, f32[6,8,64]{2,1,0:T(8,128)S(1)} %fusion.1, f32[6,8,64]{2,1,0:T(8,128)S(1)} %fusion.2, f32[8,64,320]{2,1,0:T(8,128)S(1)} %bitcast.229, f32[1,6,8,64,320]{4,3,2,1,0:T(8,128)} %concatenate.116, pred[6,320]{1,0:T(8,128)(4,1)S(1)} %add_compare_fusion), kind=kLoop, calls=%fused_computation.2 | loop fusion | flops 6878208 | bytes 8558464 | tf_op jit(solution)/shard_map/reduce_sum | solution.py:89
  74.2 5.5 %fusion.3 = (f32[8,64,320]{2,1,0:T(8,128)}, bf16[1,6,8,64,320]{4,3,2,1,0:T(8,128)(2,1)S(1)}, bf16[1,6,8,64,320]{4,3,2,1,0:T(8,128)(2,1)S(1)}) fusion(f32[1,6,8,64,320]{4,3,2,1,0:T(8,128)S(1)} %copy-done.3, f32[6,8,64]{2,1,0:T(8,128)S(1)} %multiply_reduce_fusion, f32[6,8,64]{2,1,0:T(8,128)S(1)} %fusion.1, f32[6,8,64]{2,1,0:T(8,128)S(1)} %fusion.2, ...), kind=kLoop, calls=%fused_computation.8 | loop fusion | flops 10649600 | bytes 13145984 | tf_op jit(solution)/shard_map/reduce_sum | solution.py:91
  97.3 1.8 slice.550
  101.3 2.3 %slice.537 = bf16[1,384,1024]{2,0,1:T(2,128)(2,1)} slice(f32[1,640,1024]{2,0,1:T(1,128)S(1)} %bitcast.232), slice={[0:1], [256:640], [0:1024]} | slice | bytes 1572864 | tf_op jit(solution)/shard_map/slice | solution.py:147
  103.6 2.2 %slice.548 = bf16[1,384,1024]{2,0,1:T(2,128)(2,1)} slice(f32[1,640,1024]{2,0,1:T(1,128)S(1)} %bitcast.235), slice={[0:1], [256:640], [0:1024]} | slice | bytes 1572864 | tf_op jit(solution)/shard_map/slice | solution.py:148
  107.2 2.1 %reshape.1137 = bf16[1,384,1024]{2,1,0:T(8,128)(2,1)} reshape(bf16[1,6,64,8,128]{4,3,2,1,0:T(8,128)(2,1)} %copy.104) | data formatting | bytes 1572864 | tf_op jit(solution)/shard_map/reshape | solution.py:149
  110.7 2.7 %reshape.1155 = f32[8,28608]{1,0:T(8,128)} reshape(f32[8,64,447]{2,1,0:T(8,128)} %maximum_maximum_fusion) | data formatting | bytes 1830912 | tf_op jit(solution)/shard_map/reshape | solution.py:53
  113.4 2.2 %concatenate.125 = f32[8,28672]{1,0:T(8,128)} pad(f32[8,28608]{1,0:T(8,128)} %reshape.1155, f32[]{:T(128)} %constant.322.clone.1), padding=0_0x0_64 | pad | bytes 1832964 | tf_op jit(solution)/shard_map/concatenate | solution.py:52
  115.6 2.7 %reshape.1156 = f32[8,64,448]{2,1,0:T(8,128)} reshape(f32[8,28672]{1,0:T(8,128)} %concatenate.125) | data formatting | bytes 1835008 | tf_op jit(solution)/shard_map/reshape | solution.py:55
  119.7 54.4 %psum.7 = f32[16,192]{1,0:T(8,128)} all-reduce(f32[16,192]{1,0:T(8,128)S(1)} %convolution_dynamic-update-slice_fusion), channel_id=1, replica_groups=mesh['sp'=16,'tp'=2] {'sp','tp'}, use_global_device_ids=true, to_apply=%region_5.6 | all-reduce | flops 3072 | bytes 24576 | tf_op jit(solution)/shard_map/psum | solution.py:162
  174.1 3.8 %fusion.14 = bf16[1,384,1024]{2,0,1:T(2,128)(2,1)} fusion(bf16[1,384,1024]{2,0,1:T(2,128)(2,1)} %slice.537, f32[1,256,1024]{2,0,1:T(1,128)} %collective-permute-done.2, f32[1,640,1024]{2,0,1:T(1,128)S(1)} %bitcast.233), kind=kLoop, calls=%fused_computation.46 | loop fusion | flops 262144 | bytes 3145728 | tf_op jit(solution)/shard_map/scatter-add | solution.py:147
  177.9 2.6 %copy.127 = bf16[1,384,1024]{2,1,0:T(8,128)(2,1)} copy(bf16[1,384,1024]{2,0,1:T(2,128)(2,1)} %fusion.14) | data formatting | bytes 1572864
  180.5 2.7 %fusion.13 = bf16[1,384,1024]{2,0,1:T(2,128)(2,1)S(1)} fusion(bf16[1,384,1024]{2,0,1:T(2,128)(2,1)S(1)} %copy-done.13, f32[1,256,1024]{2,0,1:T(1,128)} %collective-permute-done.3, f32[1,640,1024]{2,0,1:T(1,128)} %bitcast.236), kind=kLoop, calls=%fused_computation.44 | loop fusion | flops 262144 | bytes 3145728 | tf_op jit(solution)/shard_map/scatter-add | solution.py:148
  (95 shorter events, 49.9 us)
Async XLA Ops:
  0.6 13.0 %copy-start = (f32[8,192]{1,0:T(8,128)S(1)}, f32[8,192]{1,0:T(8,128)}, u32[]{:S(2)}) copy-start(f32[8,192]{1,0:T(8,128)} %param.32) | copy-start | bytes 18436
  0.6 13.2 %copy-start.16 = (bf16[1,384,1024]{2,1,0:T(8,128)(2,1)S(1)}, bf16[1,384,1024]{2,1,0:T(8,128)(2,1)}, u32[]{:S(2)}) copy-start(bf16[1,384,1024]{2,1,0:T(8,128)(2,1)} %param.33) | copy-start | bytes 2359300
  0.7 13.4 %copy-start.17 = (bf16[1,384,1024]{2,1,0:T(8,128)(2,1)S(1)}, bf16[1,384,1024]{2,1,0:T(8,128)(2,1)}, u32[]{:S(2)}) copy-start(bf16[1,384,1024]{2,1,0:T(8,128)(2,1)} %param.29) | copy-start | bytes 2359300
  2.7 17.5 %collective-permute-start = (bf16[1,256,1024]{2,1,0:T(8,128)(2,1)}, bf16[1,256,1024]{2,1,0:T(8,128)(2,1)}, u32[]{:S(2)}, u32[]{:S(2)}) collective-permute-start(bf16[1,256,1024]{2,1,0:T(8,128)(2,1)} %slice.478), channel_id=1, source_target_pairs={{0,2},{2,4},{4,6},{6,8},{8,10},{10,12},{12,14},{14,16},{16,18},{18... | collective-permute-start | bytes 1572872 | tf_op jit(solution)/shard_map/ppermute | solution.py:17
  10.2 20.0 %collective-permute-start.1 = (bf16[1,256,1024]{2,1,0:T(8,128)(2,1)}, bf16[1,256,1024]{2,1,0:T(8,128)(2,1)}, u32[]{:S(2)}, u32[]{:S(2)}) collective-permute-start(bf16[1,256,1024]{2,1,0:T(8,128)(2,1)} %slice.486), channel_id=1, source_target_pairs={{0,2},{2,4},{4,6},{6,8},{8,10},{10,12},{12,14},{14,16},{16,18},{18... | collective-permute-start | bytes 1572872 | tf_op jit(solution)/shard_map/ppermute | solution.py:17
  21.9 8.4 %copy-start.15 = (bf16[1,384,1024]{2,1,0:T(8,128)(2,1)S(1)}, bf16[1,384,1024]{2,1,0:T(8,128)(2,1)}, u32[]{:S(2)}) copy-start(bf16[1,384,1024]{2,1,0:T(8,128)(2,1)} %param.31) | copy-start | bytes 2359300
  22.8 20.1 %copy-start.7 = (bf16[1,6,64,8,128]{4,3,2,1,0:T(8,128)(2,1)}, bf16[1,6,64,8,128]{4,3,2,1,0:T(8,128)(2,1)S(1)}, u32[]{:S(2)}) copy-start(bf16[1,6,64,8,128]{4,3,2,1,0:T(8,128)(2,1)S(1)} %get-tuple-element.162) | copy-start | bytes 2359300
  22.8 21.8 %copy-start.9 = (bf16[1,6,64,8,128]{4,3,2,1,0:T(8,128)(2,1)}, bf16[1,6,64,8,128]{4,3,2,1,0:T(8,128)(2,1)S(1)}, u32[]{:S(2)}) copy-start(bf16[1,6,64,8,128]{4,3,2,1,0:T(8,128)(2,1)S(1)} %get-tuple-element.161) | copy-start | bytes 2359300
  22.8 23.5 %copy-start.11 = (bf16[1,6,64,8,128]{4,3,2,1,0:T(8,128)(2,1)}, bf16[1,6,64,8,128]{4,3,2,1,0:T(8,128)(2,1)S(1)}, u32[]{:S(2)}) copy-start(bf16[1,6,64,8,128]{4,3,2,1,0:T(8,128)(2,1)S(1)} %get-tuple-element.160) | copy-start | bytes 2359300
  22.8 25.3 %copy-start.5 = (bf16[1,6,64,8,128]{4,3,2,1,0:T(8,128)(2,1)}, bf16[1,6,64,8,128]{4,3,2,1,0:T(8,128)(2,1)S(1)}, u32[]{:S(2)}) copy-start(bf16[1,6,64,8,128]{4,3,2,1,0:T(8,128)(2,1)S(1)} %get-tuple-element.159) | copy-start | bytes 2359300
  56.7 3.8 %copy-start.2 = (f32[1,6,8,64,320]{4,3,2,1,0:T(8,128)S(1)}, f32[1,6,8,64,320]{4,3,2,1,0:T(8,128)}, u32[]{:S(2)}) copy-start(f32[1,6,8,64,320]{4,3,2,1,0:T(8,128)} %concatenate.116) | copy-start | bytes 11796484
  69.1 5.1 %copy-start.3 = (f32[1,6,8,64,320]{4,3,2,1,0:T(8,128)S(1)}, f32[1,6,8,64,320]{4,3,2,1,0:T(8,128)}, u32[]{:S(2)}) copy-start(f32[1,6,8,64,320]{4,3,2,1,0:T(8,128)} %concatenate.123) | copy-start | bytes 11796484
  74.2 5.5 %copy-start.12 = (bf16[1,6,64,8,128]{4,3,2,1,0:T(8,128)(2,1)S(1)}, bf16[1,6,64,8,128]{4,3,2,1,0:T(8,128)(2,1)}, u32[]{:S(2)}) copy-start(bf16[1,6,64,8,128]{4,3,2,1,0:T(8,128)(2,1)} %copy-done.11) | copy-start | bytes 2359300
  79.7 1.1 copy-start.10
  89.1 85.1 %collective-permute-start.2 = (f32[1,256,1024]{2,0,1:T(1,128)}, f32[1,256,1024]{2,0,1:T(1,128)}, u32[]{:S(2)}, u32[]{:S(2)}) collective-permute-start(f32[1,256,1024]{2,0,1:T(1,128)} %slice.539), channel_id=1, source_target_pairs={{2,0},{4,2},{6,4},{8,6},{10,8},{12,10},{14,12},{16,14},{18,16},{20... | collective-permute-start | bytes 3145736 | tf_op jit(solution)/shard_map/ppermute | solution.py:17
  94.1 1.1 copy-start.8
  97.3 6.3 %copy-start.4 = (f32[1,10,64,8,128]{4,3,0,2,1:T(8,128)}, f32[1,10,64,8,128]{4,3,0,2,1:T(8,128)S(1)}, u32[]{:S(2)}) copy-start(f32[1,10,64,8,128]{4,3,0,2,1:T(8,128)S(1)} %copy.126) | copy-start | bytes 7864324
  97.3 3.4 %copy-start.6 = (bf16[1,6,64,8,128]{4,3,2,1,0:T(8,128)(2,1)S(1)}, bf16[1,6,64,8,128]{4,3,2,1,0:T(8,128)(2,1)}, u32[]{:S(2)}) copy-start(bf16[1,6,64,8,128]{4,3,2,1,0:T(8,128)(2,1)} %copy-done.5) | copy-start | bytes 2359300
  99.1 81.4 %collective-permute-start.3 = (f32[1,256,1024]{2,0,1:T(1,128)}, f32[1,256,1024]{2,0,1:T(1,128)}, u32[]{:S(2)}, u32[]{:S(2)}) collective-permute-start(f32[1,256,1024]{2,0,1:T(1,128)} %slice.550), channel_id=1, source_target_pairs={{2,0},{4,2},{6,4},{8,6},{10,8},{12,10},{14,12},{16,14},{18,16},{20... | collective-permute-start | bytes 3145736 | tf_op jit(solution)/shard_map/ppermute | solution.py:17
  105.8 3.5 %copy-start.14 = (f32[8,64,320]{2,1,0:T(8,128)S(1)}, f32[8,64,320]{2,1,0:T(8,128)}, u32[]{:S(2)}) copy-start(f32[8,64,320]{2,1,0:T(8,128)} %get-tuple-element.156) | copy-start | bytes 1966084
  174.1 6.4 %copy-start.13 = (bf16[1,384,1024]{2,0,1:T(2,128)(2,1)S(1)}, bf16[1,384,1024]{2,0,1:T(2,128)(2,1)}, u32[]{:S(2)}) copy-start(bf16[1,384,1024]{2,0,1:T(2,128)(2,1)} %slice.548) | copy-start | bytes 2359300
  177.9 6.4 %copy-start.1 = (f32[8,192]{1,0:T(8,128)S(1)}, f32[8,192]{1,0:T(8,128)}, u32[]{:S(2)}) copy-start(f32[8,192]{1,0:T(8,128)} %param.32) | copy-start | bytes 18436
where the time goes:
time: 185 us; the launch traced here: 184 us
  blocking collectives  54.4 us (29%)
  local copies, waits for them, and re-layouts  52.7 us (28%)
  matrix products  27.5 us (15%)
  other arithmetic  27.1 us (15%)
  starting transfers between devices  12.1 us (7%)
  waiting for transfers between devices  9.53 us (5%)
    psum x1, blocking collectives, local(): bias_grad = lax.psum(full_table, ('sp', 'tp'))  54.4 us
    ppermute x4, starting transfers between devices, from_behind(): lax.ppermute(value, axis, [(source, source + steps) for source in range(l...  12.1 us
    ppermute x4, waiting for transfers between devices, from_behind(): lax.ppermute(value, axis, [(source, source + steps) for source in range(l...  9.53 us
    dot_general x5, matrix products, band_core(): jnp.einsum('sncha,snkha->snhck', q_segs, k_band[:, offset:offset + seg_co...  8.59 us
    dot_general x5, matrix products, band_core(): jnp.einsum('sncha,snkha->snhck', g_segs, v_band[:, offset:offset + seg_co...  8.5 us
    concatenate x1, local copies, waits for them, and re-layouts, band_core(): prob_grad = jnp.concatenate(prob_parts, axis=-1)  7.01 us
    concatenate x1, local copies, waits for them, and re-layouts, band_core(): jnp.concatenate(score_parts, axis=-1) * score_scale + table[None, None]  6.93 us
    unnamed x42, local copies, waits for them, and re-layouts  6.5 us
  transfers between devices with their start and end apart: 4, of which 2 were waited for; matrix products, arithmetic and copies ran while one was open for 23% of the time, Pallas kernels for 0%

commit v1 on v0

--- a/solution.py
+++ b/solution.py
@@ -159,7 +159,7 @@
     full_table = lax.dynamic_update_slice_in_dim(
         full_table, local_bias, lax.axis_index("tp") * head_count, 0
     )
-    bias_grad = lax.psum(full_table, ("sp", "tp"))
+    bias_grad = lax.psum(lax.psum(full_table, "tp"), "sp")
     return (query_grad, key_grad, value_grad, bias_grad)
 
 

time: 185 us -> 220 us (1.19)
  blocking collectives: 54.4 us -> 88.9 us
    psum x1 -> x2, blocking collectives: 54.4 us -> 88.9 us  [local(): bias_grad = lax.psum(lax.psum(full_table, 'tp'), 'sp')]
  transfers between devices with their start and end apart: 4 -> 4, of which waited for: 2 -> 2; matrix products, arithmetic and copies ran while one was open for 23% -> 19% of each run, Pallas kernels for 0% -> 0%
where the time goes in v1:
time: 220 us; the launch traced here: 219 us
  blocking collectives  88.9 us (40%)
  local copies, waits for them, and re-layouts  53 us (24%)
  matrix products  27.5 us (12%)
  other arithmetic  27.1 us (12%)
  starting transfers between devices  11.8 us (5%)
  waiting for transfers between devices  9.51 us (4%)
    psum x2, blocking collectives, local(): bias_grad = lax.psum(lax.psum(full_table, 'tp'), 'sp')  88.9 us
    ppermute x4, starting transfers between devices, from_behind(): lax.ppermute(value, axis, [(source, source + steps) for source in range(l...  11.8 us
    ppermute x4, waiting for transfers between devices, from_behind(): lax.ppermute(value, axis, [(source, source + steps) for source in range(l...  9.51 us
    dot_general x5, matrix products, band_core(): jnp.einsum('sncha,snkha->snhck', q_segs, k_band[:, offset:offset + seg_co...  8.55 us
    dot_general x5, matrix products, band_core(): jnp.einsum('sncha,snkha->snhck', g_segs, v_band[:, offset:offset + seg_co...  8.5 us
    concatenate x1, local copies, waits for them, and re-layouts, band_core(): prob_grad = jnp.concatenate(prob_parts, axis=-1)  7.01 us
    concatenate x1, local copies, waits for them, and re-layouts, band_core(): jnp.concatenate(score_parts, axis=-1) * score_scale + table[None, None]  6.94 us
    unnamed x42, local copies, waits for them, and re-layouts  6.86 us
  transfers between devices with their start and end apart: 4, of which 2 were waited for; matrix products, arithmetic and copies ran while one was open for 19% of the time, Pallas kernels for 0%

profile of v1, /device:TPU:0, one launch (start us, length us, event | category | flops | bytes accessed | tf_op | source)
XLA Modules:
  0.0 218.8 jit_solution(13255046188366286213)
XLA Ops:
  0.7 2.0 slice.478
  2.7 5.7 %collective-permute-start = (bf16[1,256,1024]{2,1,0:T(8,128)(2,1)}, bf16[1,256,1024]{2,1,0:T(8,128)(2,1)}, u32[]{:S(2)}, u32[]{:S(2)}) collective-permute-start(bf16[1,256,1024]{2,1,0:T(8,128)(2,1)} %slice.478), channel_id=1, source_target_pairs={{0,2},{2,4},{4,6},{6,8},{8,10},{10,12},{12,14},{14,16},{16,18},{18... | collective-permute-start | bytes 1572872 | tf_op jit(solution)/shard_map/ppermute | solution.py:17
  8.3 1.9 slice.486
  10.2 3.4 %collective-permute-start.1 = (bf16[1,256,1024]{2,1,0:T(8,128)(2,1)}, bf16[1,256,1024]{2,1,0:T(8,128)(2,1)}, u32[]{:S(2)}, u32[]{:S(2)}) collective-permute-start(bf16[1,256,1024]{2,1,0:T(8,128)(2,1)} %slice.486), channel_id=1, source_target_pairs={{0,2},{2,4},{4,6},{6,8},{8,10},{10,12},{12,14},{14,16},{16,18},{18... | collective-permute-start | bytes 1572872 | tf_op jit(solution)/shard_map/ppermute | solution.py:17
  16.0 2.0 reshape.1124
  18.1 2.1 collective-permute-done
  22.8 7.4 %collective-permute-done.1 = bf16[1,256,1024]{2,1,0:T(8,128)(2,1)} collective-permute-done((bf16[1,256,1024]{2,1,0:T(8,128)(2,1)}, bf16[1,256,1024]{2,1,0:T(8,128)(2,1)}, u32[]{:S(2)}, u32[]{:S(2)}) %collective-permute-start.1) | collective-permute-done | bytes 524320 | tf_op jit(solution)/shard_map/ppermute | solution.py:17
  44.5 1.8 convolution_bitcast_fusion.9
  49.7 6.9 %concatenate.116 = f32[1,6,8,64,320]{4,3,2,1,0:T(8,128)} concatenate(f32[1,6,8,64,64]{4,3,2,1,0:T(8,128)} %convolution_bitcast_fusion.11, f32[1,6,8,64,64]{4,3,2,1,0:T(8,128)} %convolution_bitcast_fusion.10, f32[1,6,8,64,64]{4,3,2,1,0:T(8,128)} %convolution_bitcast_fusion.9, f32[1,6,8,64,64]{4,3,2,1,0:T(8,128)} %convolution_bitcast_fusion.8, ...), dimensions={4} | concatenate | bytes 7864320 | tf_op jit(solution)/shard_map/concatenate | solution.py:81
  56.6 3.4 %fusion.2 = f32[6,8,64]{2,1,0:T(8,128)S(1)} fusion(f32[1,6,8,64,320]{4,3,2,1,0:T(8,128)} %concatenate.116, f32[8,64,320]{2,1,0:T(8,128)S(1)} %bitcast.227, pred[6,320]{1,0:T(8,128)(4,1)S(1)} %add_compare_fusion), kind=kLoop, calls=%fused_computation.7 | loop fusion | flops 3929088 | bytes 4601728 | tf_op jit(solution)/shard_map/reduce_max | solution.py:83
  62.0 7.0 %concatenate.123 = f32[1,6,8,64,320]{4,3,2,1,0:T(8,128)} concatenate(f32[1,6,8,64,64]{4,3,2,1,0:T(8,128)} %convolution_bitcast_fusion.6, f32[1,6,8,64,64]{4,3,2,1,0:T(8,128)} %convolution_bitcast_fusion.5, f32[1,6,8,64,64]{4,3,2,1,0:T(8,128)} %convolution_bitcast_fusion.4, f32[1,6,8,64,64]{4,3,2,1,0:T(8,128)} %convolution_bitcast_fusion.3, ...), dimensions={4} | concatenate | bytes 7864320 | tf_op jit(solution)/shard_map/concatenate | solution.py:88
  69.0 4.9 %multiply_reduce_fusion = f32[6,8,64]{2,1,0:T(8,128)S(1)} fusion(f32[1,6,8,64,320]{4,3,2,1,0:T(8,128)} %concatenate.123, f32[6,8,64]{2,1,0:T(8,128)S(1)} %fusion.1, f32[6,8,64]{2,1,0:T(8,128)S(1)} %fusion.2, f32[8,64,320]{2,1,0:T(8,128)S(1)} %bitcast.229, f32[1,6,8,64,320]{4,3,2,1,0:T(8,128)} %concatenate.116, pred[6,320]{1,0:T(8,128)(4,1)S(1)} %add_compare_fusion), kind=kLoop, calls=%fused_computation.2 | loop fusion | flops 6878208 | bytes 8558464 | tf_op jit(solution)/shard_map/reduce_sum | solution.py:89
  74.1 5.5 %fusion.3 = (f32[8,64,320]{2,1,0:T(8,128)}, bf16[1,6,8,64,320]{4,3,2,1,0:T(8,128)(2,1)S(1)}, bf16[1,6,8,64,320]{4,3,2,1,0:T(8,128)(2,1)S(1)}) fusion(f32[1,6,8,64,320]{4,3,2,1,0:T(8,128)S(1)} %copy-done.3, f32[6,8,64]{2,1,0:T(8,128)S(1)} %multiply_reduce_fusion, f32[6,8,64]{2,1,0:T(8,128)S(1)} %fusion.1, f32[6,8,64]{2,1,0:T(8,128)S(1)} %fusion.2, ...), kind=kLoop, calls=%fused_computation.8 | loop fusion | flops 10649600 | bytes 13145984 | tf_op jit(solution)/shard_map/reduce_sum | solution.py:91
  101.3 2.3 %slice.537 = bf16[1,384,1024]{2,0,1:T(2,128)(2,1)} slice(f32[1,640,1024]{2,0,1:T(1,128)S(1)} %bitcast.232), slice={[0:1], [256:640], [0:1024]} | slice | bytes 1572864 | tf_op jit(solution)/shard_map/slice | solution.py:147
  103.6 2.2 %slice.548 = bf16[1,384,1024]{2,0,1:T(2,128)(2,1)} slice(f32[1,640,1024]{2,0,1:T(1,128)S(1)} %bitcast.235), slice={[0:1], [256:640], [0:1024]} | slice | bytes 1572864 | tf_op jit(solution)/shard_map/slice | solution.py:148
  107.2 2.1 reshape.1137
  110.7 2.7 %reshape.1155 = f32[8,28608]{1,0:T(8,128)} reshape(f32[8,64,447]{2,1,0:T(8,128)} %maximum_maximum_fusion) | data formatting | bytes 1830912 | tf_op jit(solution)/shard_map/reshape | solution.py:53
  113.4 2.2 concatenate.125
  115.6 2.7 %reshape.1156 = f32[8,64,448]{2,1,0:T(8,128)} reshape(f32[8,28672]{1,0:T(8,128)} %concatenate.125) | data formatting | bytes 1835008 | tf_op jit(solution)/shard_map/reshape | solution.py:55
  119.7 3.4 %psum.14 = f32[16,192]{1,0:T(8,128)S(1)} all-reduce(f32[16,192]{1,0:T(8,128)S(1)} %convolution_dynamic-update-slice_fusion), channel_id=1, replica_groups=mesh['sp'=16,'tp'=2] {'tp'}, use_global_device_ids=true, to_apply=%region_5.6 | all-reduce | flops 3072 | bytes 24576 | tf_op jit(solution)/shard_map/psum | solution.py:162
  123.1 85.5 %psum.15 = f32[16,192]{1,0:T(8,128)} all-reduce(f32[16,192]{1,0:T(8,128)S(1)} %psum.14), channel_id=1, replica_groups=mesh['sp'=16,'tp'=2] {'sp'}, use_global_device_ids=true, to_apply=%region_6.7 | all-reduce | flops 3072 | bytes 24576 | tf_op jit(solution)/shard_map/psum | solution.py:162
  208.6 3.8 %fusion.14 = bf16[1,384,1024]{2,0,1:T(2,128)(2,1)} fusion(bf16[1,384,1024]{2,0,1:T(2,128)(2,1)} %slice.537, f32[1,256,1024]{2,0,1:T(1,128)} %collective-permute-done.2, f32[1,640,1024]{2,0,1:T(1,128)S(1)} %bitcast.233), kind=kLoop, calls=%fused_computation.46 | loop fusion | flops 262144 | bytes 3145728 | tf_op jit(solution)/shard_map/scatter-add | solution.py:147
  212.4 2.6 %copy.127 = bf16[1,384,1024]{2,1,0:T(8,128)(2,1)} copy(bf16[1,384,1024]{2,0,1:T(2,128)(2,1)} %fusion.14) | data formatting | bytes 1572864
  215.0 2.7 %fusion.13 = bf16[1,384,1024]{2,0,1:T(2,128)(2,1)S(1)} fusion(bf16[1,384,1024]{2,0,1:T(2,128)(2,1)S(1)} %copy-done.13, f32[1,256,1024]{2,0,1:T(1,128)} %collective-permute-done.3, f32[1,640,1024]{2,0,1:T(1,128)} %bitcast.236), kind=kLoop, calls=%fused_computation.44 | loop fusion | flops 262144 | bytes 3145728 | tf_op jit(solution)/shard_map/scatter-add | solution.py:148
  (96 shorter events, 51.7 us)
Async XLA Ops:
  0.6 13.0 %copy-start = (f32[8,192]{1,0:T(8,128)S(1)}, f32[8,192]{1,0:T(8,128)}, u32[]{:S(2)}) copy-start(f32[8,192]{1,0:T(8,128)} %param.32) | copy-start | bytes 18436
  0.6 13.3 %copy-start.16 = (bf16[1,384,1024]{2,1,0:T(8,128)(2,1)S(1)}, bf16[1,384,1024]{2,1,0:T(8,128)(2,1)}, u32[]{:S(2)}) copy-start(bf16[1,384,1024]{2,1,0:T(8,128)(2,1)} %param.33) | copy-start | bytes 2359300
  0.7 13.4 %copy-start.17 = (bf16[1,384,1024]{2,1,0:T(8,128)(2,1)S(1)}, bf16[1,384,1024]{2,1,0:T(8,128)(2,1)}, u32[]{:S(2)}) copy-start(bf16[1,384,1024]{2,1,0:T(8,128)(2,1)} %param.29) | copy-start | bytes 2359300
  2.7 17.5 %collective-permute-start = (bf16[1,256,1024]{2,1,0:T(8,128)(2,1)}, bf16[1,256,1024]{2,1,0:T(8,128)(2,1)}, u32[]{:S(2)}, u32[]{:S(2)}) collective-permute-start(bf16[1,256,1024]{2,1,0:T(8,128)(2,1)} %slice.478), channel_id=1, source_target_pairs={{0,2},{2,4},{4,6},{6,8},{8,10},{10,12},{12,14},{14,16},{16,18},{18... | collective-permute-start | bytes 1572872 | tf_op jit(solution)/shard_map/ppermute | solution.py:17
  10.2 20.0 %collective-permute-start.1 = (bf16[1,256,1024]{2,1,0:T(8,128)(2,1)}, bf16[1,256,1024]{2,1,0:T(8,128)(2,1)}, u32[]{:S(2)}, u32[]{:S(2)}) collective-permute-start(bf16[1,256,1024]{2,1,0:T(8,128)(2,1)} %slice.486), channel_id=1, source_target_pairs={{0,2},{2,4},{4,6},{6,8},{8,10},{10,12},{12,14},{14,16},{16,18},{18... | collective-permute-start | bytes 1572872 | tf_op jit(solution)/shard_map/ppermute | solution.py:17
  21.9 8.4 %copy-start.15 = (bf16[1,384,1024]{2,1,0:T(8,128)(2,1)S(1)}, bf16[1,384,1024]{2,1,0:T(8,128)(2,1)}, u32[]{:S(2)}) copy-start(bf16[1,384,1024]{2,1,0:T(8,128)(2,1)} %param.31) | copy-start | bytes 2359300
  22.8 18.4 %copy-start.7 = (bf16[1,6,64,8,128]{4,3,2,1,0:T(8,128)(2,1)}, bf16[1,6,64,8,128]{4,3,2,1,0:T(8,128)(2,1)S(1)}, u32[]{:S(2)}) copy-start(bf16[1,6,64,8,128]{4,3,2,1,0:T(8,128)(2,1)S(1)} %get-tuple-element.163) | copy-start | bytes 2359300
  22.8 21.8 %copy-start.9 = (bf16[1,6,64,8,128]{4,3,2,1,0:T(8,128)(2,1)}, bf16[1,6,64,8,128]{4,3,2,1,0:T(8,128)(2,1)S(1)}, u32[]{:S(2)}) copy-start(bf16[1,6,64,8,128]{4,3,2,1,0:T(8,128)(2,1)S(1)} %get-tuple-element.161) | copy-start | bytes 2359300
  22.8 23.5 %copy-start.11 = (bf16[1,6,64,8,128]{4,3,2,1,0:T(8,128)(2,1)}, bf16[1,6,64,8,128]{4,3,2,1,0:T(8,128)(2,1)S(1)}, u32[]{:S(2)}) copy-start(bf16[1,6,64,8,128]{4,3,2,1,0:T(8,128)(2,1)S(1)} %get-tuple-element.160) | copy-start | bytes 2359300
  22.8 25.2 %copy-start.5 = (bf16[1,6,64,8,128]{4,3,2,1,0:T(8,128)(2,1)}, bf16[1,6,64,8,128]{4,3,2,1,0:T(8,128)(2,1)S(1)}, u32[]{:S(2)}) copy-start(bf16[1,6,64,8,128]{4,3,2,1,0:T(8,128)(2,1)S(1)} %get-tuple-element.159) | copy-start | bytes 2359300
  56.6 3.8 %copy-start.2 = (f32[1,6,8,64,320]{4,3,2,1,0:T(8,128)S(1)}, f32[1,6,8,64,320]{4,3,2,1,0:T(8,128)}, u32[]{:S(2)}) copy-start(f32[1,6,8,64,320]{4,3,2,1,0:T(8,128)} %concatenate.116) | copy-start | bytes 11796484
  69.0 5.1 %copy-start.3 = (f32[1,6,8,64,320]{4,3,2,1,0:T(8,128)S(1)}, f32[1,6,8,64,320]{4,3,2,1,0:T(8,128)}, u32[]{:S(2)}) copy-start(f32[1,6,8,64,320]{4,3,2,1,0:T(8,128)} %concatenate.123) | copy-start | bytes 11796484
  74.1 5.5 %copy-start.12 = (bf16[1,6,64,8,128]{4,3,2,1,0:T(8,128)(2,1)S(1)}, bf16[1,6,64,8,128]{4,3,2,1,0:T(8,128)(2,1)}, u32[]{:S(2)}) copy-start(bf16[1,6,64,8,128]{4,3,2,1,0:T(8,128)(2,1)} %copy-done.11) | copy-start | bytes 2359300
  79.6 1.1 copy-start.10
  80.8 1.1 copy-start.8
  90.3 118.3 %collective-permute-start.2 = (f32[1,256,1024]{2,0,1:T(1,128)}, f32[1,256,1024]{2,0,1:T(1,128)}, u32[]{:S(2)}, u32[]{:S(2)}) collective-permute-start(f32[1,256,1024]{2,0,1:T(1,128)} %slice.539), channel_id=1, source_target_pairs={{2,0},{4,2},{6,4},{8,6},{10,8},{12,10},{14,12},{16,14},{18,16},{20... | collective-permute-start | bytes 3145736 | tf_op jit(solution)/shard_map/ppermute | solution.py:17
  97.6 5.9 %copy-start.4 = (f32[1,10,64,8,128]{4,3,0,2,1:T(8,128)}, f32[1,10,64,8,128]{4,3,0,2,1:T(8,128)S(1)}, u32[]{:S(2)}) copy-start(f32[1,10,64,8,128]{4,3,0,2,1:T(8,128)S(1)} %copy.126) | copy-start | bytes 7864324
  97.6 3.0 %copy-start.6 = (bf16[1,6,64,8,128]{4,3,2,1,0:T(8,128)(2,1)S(1)}, bf16[1,6,64,8,128]{4,3,2,1,0:T(8,128)(2,1)}, u32[]{:S(2)}) copy-start(bf16[1,6,64,8,128]{4,3,2,1,0:T(8,128)(2,1)} %copy-done.5) | copy-start | bytes 2359300
  99.3 115.6 %collective-permute-start.3 = (f32[1,256,1024]{2,0,1:T(1,128)}, f32[1,256,1024]{2,0,1:T(1,128)}, u32[]{:S(2)}, u32[]{:S(2)}) collective-permute-start(f32[1,256,1024]{2,0,1:T(1,128)} %slice.550), channel_id=1, source_target_pairs={{2,0},{4,2},{6,4},{8,6},{10,8},{12,10},{14,12},{16,14},{18,16},{20... | collective-permute-start | bytes 3145736 | tf_op jit(solution)/shard_map/ppermute | solution.py:17
  105.8 3.5 %copy-start.14 = (f32[8,64,320]{2,1,0:T(8,128)S(1)}, f32[8,64,320]{2,1,0:T(8,128)}, u32[]{:S(2)}) copy-start(f32[8,64,320]{2,1,0:T(8,128)} %get-tuple-element.156) | copy-start | bytes 1966084
  208.6 6.4 %copy-start.13 = (bf16[1,384,1024]{2,0,1:T(2,128)(2,1)S(1)}, bf16[1,384,1024]{2,0,1:T(2,128)(2,1)}, u32[]{:S(2)}) copy-start(bf16[1,384,1024]{2,0,1:T(2,128)(2,1)} %slice.548) | copy-start | bytes 2359300
  212.4 6.4 %copy-start.1 = (f32[8,192]{1,0:T(8,128)S(1)}, f32[8,192]{1,0:T(8,128)}, u32[]{:S(2)}) copy-start(f32[8,192]{1,0:T(8,128)} %param.32) | copy-start | bytes 18436
